TPU v7x, 32 devices: a whole 2x2x4 slice. The times are simulated.
32 devices in a mesh: fs: 4 (over z), rep: 2 (over y), tp: 4 (over x, core).
Axes of the slice: x: 2, y: 2, z: 4, core: 2. Of those that a mesh axis runs over, the one named last changes fastest.
Arguments:
- saved_input: bfloat16 [5120, 3072], P(('fs', 'rep')), may hold values from -6 to 6
- key_cotangent: bfloat16 [5120, 1024], P(('fs', 'rep'), 'tp'), may hold values from -0.0625 to 0.0625
- value_cotangent: bfloat16 [5120, 2048], P(('fs', 'rep'), 'tp'), may hold values from -0.0625 to 0.0625
- key_factor: bfloat16 [3072, 256], replicated, may hold values from -0.375 to 0.375
- value_factor: bfloat16 [3072, 256], replicated, may hold values from -0.375 to 0.375
- key_weight: float32 [3072, 1024], P(('fs', 'rep'), 'tp'), may hold values from -0.109375 to 0.109375
- value_weight: float32 [3072, 2048], P(('fs', 'rep'), 'tp'), may hold values from -0.109375 to 0.109375
- key_first: float32 [256, 1024], P(None, 'tp'), as said below
- key_second: float32 [256, 1024], P(None, 'tp'), may hold values from 0.05 to 1
- value_first: float32 [256, 2048], P(None, 'tp'), as said below
- value_second: float32 [256, 2048], P(None, 'tp'), may hold values from 0.05 to 1
Outputs:
- key_weight_new: float32 [3072, 1024], P(('fs', 'rep'), 'tp')
- value_weight_new: float32 [3072, 2048], P(('fs', 'rep'), 'tp')
- key_first_new: float32 [256, 1024], P(None, 'tp')
- key_second_new: float32 [256, 1024], P(None, 'tp')
- value_first_new: float32 [256, 2048], P(None, 'tp')
- value_second_new: float32 [256, 2048], P(None, 'tp')
- key_step: float32 [3072, 1024], P(('fs', 'rep'), 'tp')
- value_step: float32 [3072, 2048], P(('fs', 'rep'), 'tp')
- key_copy: bfloat16 [3072, 1024], P(None, 'tp')
- value_copy: bfloat16 [3072, 2048], P(None, 'tp')
Inputs may be any that keep to these rules, and one draw needn't show every extreme that they name: `key_first`: real-valued moments whose scale differs from head to head. `value_first`: real-valued moments whose scale differs from head to head.
All inputs are finite; a program needn't handle non-finite values.
Results may differ from a plain program's by a relative error of at most 0.004.
Values may be sent and summed in bfloat16 or wider, within the bound.
No kernel may reach another device: no remote copies, remote signals or barrier semaphores. Data moves between devices by JAX's collectives and lax.ppermute only.
A program may use at most 64 MiB of HBM per device.

v0:
```python
import jax
import jax.numpy as jnp
from jax import lax
from jax.sharding import PartitionSpec as P

DK = 1024
DV = 2048
RK = 256
RV = 256
first_decay = 0.8
second_decay = 0.9
epsilon = 1e-08
learn_rate = 0.01


def split_contract(basis, cotangent):
    upper = basis.astype(jnp.bfloat16)
    lower = (basis - upper.astype(jnp.float32)).astype(jnp.bfloat16)
    dims = (((0,), (0,)), ((), ()))
    high_part = lax.dot_general(upper, cotangent, dims, preferred_element_type=jnp.float32)
    low_part = lax.dot_general(lower, cotangent, dims, preferred_element_type=jnp.float32)
    return high_part + low_part


def moments(projection, first, second):
    first_new = first_decay * first + (1.0 - first_decay) * projection
    second_new = second_decay * second + (1.0 - second_decay) * projection * projection
    normed = first_new / (jnp.sqrt(second_new) + epsilon)
    return (first_new, second_new, normed)


def body(
    saved_input,
    key_cotangent,
    value_cotangent,
    key_factor,
    value_factor,
    key_weight,
    value_weight,
    key_first,
    key_second,
    value_first,
    value_second,
):
    local_rows = key_weight.shape[0]
    row_offset = lax.axis_index(("fs", "rep")) * local_rows
    key_rows = lax.dynamic_slice_in_dim(key_factor, row_offset, local_rows, 0).astype(jnp.float32)
    value_rows = lax.dynamic_slice_in_dim(value_factor, row_offset, local_rows, 0).astype(
        jnp.float32
    )
    key_basis = jnp.dot(saved_input, key_factor, preferred_element_type=jnp.float32)
    key_part = split_contract(key_basis, key_cotangent)
    value_basis = jnp.dot(saved_input, value_factor, preferred_element_type=jnp.float32)
    value_part = split_contract(value_basis, value_cotangent)
    key_projected, value_projected = lax.psum((key_part, value_part), ("fs", "rep"))
    key_first_new, key_second_new, key_normed = moments(key_projected, key_first, key_second)
    value_first_new, value_second_new, value_normed = moments(
        value_projected, value_first, value_second
    )
    local_squares = jnp.sum(key_normed * key_normed) + jnp.sum(value_normed * value_normed)
    squares = lax.psum(local_squares, "tp")
    entries = jnp.float32(RK * DK + RV * DV)
    shrink = jnp.sqrt(entries / (entries + squares))
    key_step = shrink * jnp.dot(key_rows, key_normed, precision=lax.Precision.HIGHEST)
    value_step = shrink * jnp.dot(value_rows, value_normed, precision=lax.Precision.HIGHEST)
    key_weight_new = key_weight - learn_rate * key_step
    value_weight_new = value_weight - learn_rate * value_step
    key_copy, value_copy = (
        lax.all_gather(key_weight_new.astype(jnp.bfloat16), ("fs", "rep"), axis=0, tiled=True),
        lax.all_gather(value_weight_new.astype(jnp.bfloat16), ("fs", "rep"), axis=0, tiled=True),
    )
    return (
        key_weight_new,
        value_weight_new,
        key_first_new,
        key_second_new,
        value_first_new,
        value_second_new,
        key_step,
        value_step,
        key_copy,
        value_copy,
    )


def solution(mesh):
    in_specs = (
        P(("fs", "rep"), None),
        P(("fs", "rep"), "tp"),
        P(("fs", "rep"), "tp"),
        P(),
        P(),
        P(("fs", "rep"), "tp"),
        P(("fs", "rep"), "tp"),
        P(None, "tp"),
        P(None, "tp"),
        P(None, "tp"),
        P(None, "tp"),
    )
    out_specs = (
        P(("fs", "rep"), "tp"),
        P(("fs", "rep"), "tp"),
        P(None, "tp"),
        P(None, "tp"),
        P(None, "tp"),
        P(None, "tp"),
        P(("fs", "rep"), "tp"),
        P(("fs", "rep"), "tp"),
        P(None, "tp"),
        P(None, "tp"),
    )
    return jax.shard_map(body, mesh=mesh, in_specs=in_specs, out_specs=out_specs, check_vma=False)
```

profile of v0, /device:TPU:0, one launch (start us, length us, event | category | flops | bytes accessed | tf_op | source)
XLA Modules:
  0.0 225.4 jit_solution(12211310105299718607)
XLA Ops:
  7.2 0.0 copy-start
  7.2 0.0 copy-start.2
  7.2 0.0 all-reduce.3.cloned.1.call-start
  7.2 1.3 copy-done
  8.6 0.0 copy-start.12
  8.6 3.4 %fusion.17 = f32[640,256]{1,0:T(8,128)S(1)} fusion(bf16[640,3072]{1,0:T(8,128)(2,1)} %param.11, bf16[3072,256]{1,0:T(8,128)(2,1)S(1)} %copy-done), kind=kOutput, calls=%fused_computation.31 | convolution fusion | flops 1006632960 | bytes 6160384 | tf_op jit(solution)/shard_map/dot_general | solution.py:53
  12.0 0.0 copy-done.2
  12.1 0.4 fusion.5
  12.5 0.0 copy-start.11
  12.5 1.2 convolution_add_fusion
  13.7 0.0 copy-done.12
  13.7 0.3 copy-done.11
  13.9 0.0 copy-start.5
  13.9 1.2 fusion.16
  15.1 0.0 copy-done.5
  15.1 0.0 copy-start.8
  15.2 0.3 fusion.8
  15.5 1.0 convolution_add_fusion.1
  16.5 0.0 all-reduce.3.cloned.1.call-update
  16.5 0.0 all-gather.3.cloned.1.call-start
  16.6 77.9 %all-reduce.3.cloned.1.call-done = (f32[256,256]{1,0:T(8,128)}, f32[256,512]{1,0:T(8,128)}) async-done(((f32[256,256]{1,0:T(8,128)}, f32[256,512]{1,0:T(8,128)}), (f32[256,256]{1,0:T(8,128)}, f32[256,512]{1,0:T(8,128)})) %all-reduce.3.cloned.1.call-update) | async-done | bytes 786448 | tf_op jit(solution)/shard_map/psum | solution.py:55
  94.5 0.0 copy-start.10
  94.5 0.0 copy-done.8
  94.5 0.0 copy-start.9
  94.5 2.2 multiply_reduce_fusion
  96.7 0.0 copy-start.3
  96.7 0.0 copy-start.4
  96.7 0.0 copy-done.10
  96.7 2.2 multiply_reduce_fusion.1
  98.9 0.0 copy-start.6
  98.9 0.0 copy-start.7
  100.2 6.2 %psum.23 = f32[]{:T(128)} all-reduce(f32[]{:T(128)S(6)} %add.59), channel_id=1, replica_groups=mesh['fs'=4,'rep'=2,'tp'=4] {'tp'}, use_global_device_ids=true, to_apply=%region_4.0 | all-reduce | flops 1 | bytes 8 | tf_op jit(solution)/shard_map/psum | solution.py:61
  107.1 0.0 copy-done.9
  107.1 2.3 %fusion.13 = (bf16[384,256]{1,0:T(8,128)(2,1)}, f32[384,256]{1,0:T(8,128)}, f32[384,256]{1,0:T(8,128)}) fusion(f32[384,256]{1,0:T(8,128)S(1)} %copy-done.9, f32[256,256]{1,0:T(8,128)S(1)} %get-tuple-element.36, f32[256,256]{1,0:T(8,128)S(1)} %get-tuple-element.37, bf16[3072,256]{1,0:T(8,128)(2,1)} %param.14, s32[]{:T(128)S(6)} %select_n.4, f32[]{:T(128)S(6)} %sqrt.11), kind=kOutput, calls=%fused_computation.29 | convolution fusion | flops 302514176 | bytes 2097160 | tf_op jit(solution)/shard_map/dot_general | solution.py:64
  109.4 0.0 all-gather.3.cloned.1.call-update
  109.5 0.0 all-gather.5.cloned.1.call-start
  109.5 0.0 copy-done.3
  109.5 0.0 copy-done.4
  109.5 3.2 %fusion.12 = (bf16[384,512]{1,0:T(8,128)(2,1)}, f32[384,512]{1,0:T(8,128)}, f32[384,512]{1,0:T(8,128)}) fusion(f32[384,512]{1,0:T(8,128)} %param.17, f32[256,512]{1,0:T(8,128)S(1)} %get-tuple-element.38, f32[256,512]{1,0:T(8,128)S(1)} %get-tuple-element.39, bf16[3072,256]{1,0:T(8,128)(2,1)S(1)} %copy-done, s32[]{:T(128)S(6)} %select_n.4, f32[]{:T(128)S(6)} %sqrt.11), kind=kOutput, calls=%fused_computation.28 | convolution fusion | flops 605028352 | bytes 3997704 | tf_op jit(solution)/shard_map/dot_general | solution.py:65
  112.7 0.0 copy-done.6
  112.7 0.0 copy-done.7
  112.7 0.0 all-gather.5.cloned.1.call-update
  112.7 40.5 %all-gather.3.cloned.1.call-done = bf16[3072,256]{1,0:T(8,128)(2,1)} async-done(((bf16[384,256]{1,0:T(8,128)(2,1)}), bf16[3072,256]{1,0:T(8,128)(2,1)}) %all-gather.3.cloned.1.call-update) | async-done | bytes 1572880 | tf_op jit(solution)/shard_map/all_gather | solution.py:69
  153.2 61.2 %all-gather.5.cloned.1.call-done = bf16[3072,512]{1,0:T(8,128)(2,1)} async-done(((bf16[384,512]{1,0:T(8,128)(2,1)}), bf16[3072,512]{1,0:T(8,128)(2,1)}) %all-gather.5.cloned.1.call-update) | async-done | bytes 3145744 | tf_op jit(solution)/shard_map/all_gather | solution.py:70
  214.4 0.0 copy-start.1
  214.4 2.8 %copy.25 = bf16[3072,256]{1,0:T(8,128)(2,1)} copy(bf16[3072,256]{1,0:T(8,128)(2,1)} %all-gather.3.cloned.1.call-done) | data formatting | bytes 3145728
  217.2 0.0 copy-done.1
  217.2 1.7 copy.26
Async XLA Ops:
  7.2 1.4 copy-start
  7.2 4.9 %copy-start.2 = (bf16[640,512]{1,0:T(8,128)(2,1)S(1)}, bf16[640,512]{1,0:T(8,128)(2,1)}, u32[]{:S(2)}) copy-start(bf16[640,512]{1,0:T(8,128)(2,1)} %param.13) | copy-start | bytes 1966084
  7.2 87.3 %all-reduce.3.cloned.1.call-start = ((), (), s32[]{:S(2)}) async-start(), calls=%async_computation.2 | async-start | bytes 1572864 | tf_op jit(solution)/shard_map/psum | solution.py:55
  8.6 5.1 %copy-start.12 = (bf16[640,3072]{1,0:T(8,128)(2,1)S(1)}, bf16[640,3072]{1,0:T(8,128)(2,1)}, u32[]{:S(2)}) copy-start(bf16[640,3072]{1,0:T(8,128)(2,1)} %param.11) | copy-start | bytes 11796484
  12.5 1.5 copy-start.11
  13.9 1.2 copy-start.5
  15.1 79.4 %copy-start.8 = (f32[256,512]{1,0:T(8,128)S(1)}, f32[256,512]{1,0:T(8,128)}, u32[]{:S(2)}) copy-start(f32[256,512]{1,0:T(8,128)} %param.21) | copy-start | bytes 1572868
  16.5 136.7 %all-gather.3.cloned.1.call-start = ((), (), s32[]{:S(2)}) async-start(), calls=%async_computation | async-start | bytes 1769472 | tf_op jit(solution)/shard_map/all_gather | solution.py:69
  94.5 2.2 copy-start.10
  94.5 12.6 %copy-start.9 = (f32[384,256]{1,0:T(8,128)S(1)}, f32[384,256]{1,0:T(8,128)}, u32[]{:S(2)}) copy-start(f32[384,256]{1,0:T(8,128)} %param.16) | copy-start | bytes 1179652
  96.7 12.8 %copy-start.3 = (f32[256,512]{1,0:T(8,128)}, f32[256,512]{1,0:T(8,128)S(1)}, u32[]{:S(2)}) copy-start(f32[256,512]{1,0:T(8,128)S(1)} %get-tuple-element.39) | copy-start | bytes 1572868
  96.7 12.8 %copy-start.4 = (f32[256,512]{1,0:T(8,128)}, f32[256,512]{1,0:T(8,128)S(1)}, u32[]{:S(2)}) copy-start(f32[256,512]{1,0:T(8,128)S(1)} %get-tuple-element.38) | copy-start | bytes 1572868
  98.9 13.8 %copy-start.6 = (f32[256,256]{1,0:T(8,128)}, f32[256,256]{1,0:T(8,128)S(1)}, u32[]{:S(2)}) copy-start(f32[256,256]{1,0:T(8,128)S(1)} %get-tuple-element.37) | copy-start | bytes 786436
  98.9 13.8 %copy-start.7 = (f32[256,256]{1,0:T(8,128)}, f32[256,256]{1,0:T(8,128)S(1)}, u32[]{:S(2)}) copy-start(f32[256,256]{1,0:T(8,128)S(1)} %get-tuple-element.36) | copy-start | bytes 786436
  109.5 104.9 %all-gather.5.cloned.1.call-start = ((), (), s32[]{:S(2)}) async-start(), calls=%async_computation.1 | async-start | bytes 3538944 | tf_op jit(solution)/shard_map/all_gather | solution.py:70
  214.4 2.8 %copy-start.1 = (bf16[3072,512]{1,0:T(8,128)(2,1)S(1)}, bf16[3072,512]{1,0:T(8,128)(2,1)}, u32[]{:S(2)}) copy-start(bf16[3072,512]{1,0:T(8,128)(2,1)} %all-gather.5.cloned.1.call-done) | copy-start | bytes 9437188
Sparse Core Ops, SparseCore 0:
  16.6 77.8 all-reduce.2
  109.6 43.5 all-gather.2
  156.0 58.3 all-gather.4
where the time goes:
time: 226 us; the launch traced here: 225 us
  waiting for transfers between devices  180 us (80%)
  between operations  15.9 us (7%)
  matrix products  13 us (6%)
  blocking collectives  6.17 us (3%)
  local copies, waits for them, and re-layouts  6.12 us (3%)
  other arithmetic  4.39 us (2%)
    psum x1, waiting for transfers between devices, body(): lax.psum((key_part, value_part), ('fs', 'rep'))  77.9 us
    all_gather x1, waiting for transfers between devices, body(): lax.all_gather(value_weight_new.astype(jnp.bfloat16), ('fs', 'rep'), axis...  61.2 us
    all_gather x1, waiting for transfers between devices, body(): lax.all_gather(key_weight_new.astype(jnp.bfloat16), ('fs', 'rep'), axis=0...  40.5 us
    psum x1, blocking collectives, body(): squares = lax.psum(local_squares, 'tp')  6.17 us
    unnamed x28, local copies, waits for them, and re-layouts  6.12 us
  transfers between devices with their start and end apart: 3, of which 3 were waited for; matrix products, arithmetic and copies ran while one was open for 1% of the time, Pallas kernels for 0%

commit v1 on v0

--- a/solution.py
+++ b/solution.py
@@ -11,6 +11,19 @@
 second_decay = 0.9
 epsilon = 1e-08
 learn_rate = 0.01
+
+
+def collect(x, axis, dim):
+    ways = lax.axis_size(axis)
+    up = [(d, (d + 1) % ways) for d in range(ways)]
+    down = [(d, (d - 1) % ways) for d in range(ways)]
+    earlier, later = ([x], [x])
+    for _ in range(ways // 2):
+        earlier.append(lax.ppermute(earlier[-1], axis, up))
+    for _ in range((ways - 1) // 2):
+        later.append(lax.ppermute(later[-1], axis, down))
+    line = jnp.concatenate([*earlier[::-1], *later[1:]], axis=dim)
+    return jnp.roll(line, (lax.axis_index(axis) - ways // 2) * x.shape[dim], axis=dim)
 
 
 def split_contract(basis, cotangent):
@@ -66,7 +79,7 @@
     key_weight_new = key_weight - learn_rate * key_step
     value_weight_new = value_weight - learn_rate * value_step
     key_copy, value_copy = (
-        lax.all_gather(key_weight_new.astype(jnp.bfloat16), ("fs", "rep"), axis=0, tiled=True),
+        collect(key_weight_new.astype(jnp.bfloat16), ("fs", "rep"), 0),
         lax.all_gather(value_weight_new.astype(jnp.bfloat16), ("fs", "rep"), axis=0, tiled=True),
     )
     return (

time: 226 us -> 192 us (0.85)
  waiting for transfers between devices: 180 us -> 131 us
  starting transfers between devices: 0.12 us -> 14 us
    all_gather x1, waiting for transfers between devices: 61.2 us -> 20.2 us  [body(): lax.all_gather(value_weight_new.astype(jnp.bfloat16), ('fs', 'rep'), axis...]
    all_gather x1 -> x0, waiting for transfers between devices: 40.5 us -> none  [body(): lax.all_gather(key_weight_new.astype(jnp.bfloat16), ('fs', 'rep'), axis=0...]
    ppermute x0 -> x7, waiting for transfers between devices: none -> 32.7 us  [the longest x4 26.2 us: collect(): earlier.append(lax.ppermute(earlier[-1], axis, up))]
    ppermute x0 -> x7, starting transfers between devices: none -> 13.9 us  [the longest x3 11.7 us: collect(): later.append(lax.ppermute(later[-1], axis, down))]
    unnamed x28 -> x36, local copies, waits for them, and re-layouts: 6.12 us -> 5.37 us
  transfers between devices with their start and end apart: 3 -> 9, of which waited for: 3 -> 8; matrix products, arithmetic and copies ran while one was open for 1% -> 2% of each run, Pallas kernels for 0% -> 0%
where the time goes in v1:
time: 192 us
  waiting for transfers between devices  131 us (68%)
  between operations  16.3 us (8%)
  starting transfers between devices  14 us (7%)
  matrix products  13.1 us (7%)
  local copies, waits for them, and re-layouts  6.93 us (4%)
  blocking collectives  6.17 us (3%)
  other arithmetic  4.4 us (2%)
    psum x1, waiting for transfers between devices, body(): lax.psum((key_part, value_part), ('fs', 'rep'))  78.1 us
    ppermute x4, waiting for transfers between devices, collect(): earlier.append(lax.ppermute(earlier[-1], axis, up))  26.2 us
    all_gather x1, waiting for transfers between devices, body(): lax.all_gather(value_weight_new.astype(jnp.bfloat16), ('fs', 'rep'), axis...  20.2 us
    ppermute x3, starting transfers between devices, collect(): later.append(lax.ppermute(later[-1], axis, down))  11.7 us
    ppermute x3, waiting for transfers between devices, collect(): later.append(lax.ppermute(later[-1], axis, down))  6.55 us
    psum x1, blocking collectives, body(): squares = lax.psum(local_squares, 'tp')  6.17 us
    unnamed x36, local copies, waits for them, and re-layouts  5.37 us
  transfers between devices with their start and end apart: 9, of which 8 were waited for; matrix products, arithmetic and copies ran while one was open for 2% of the time, Pallas kernels for 0%

profile of v1, /device:TPU:0, one launch (start us, length us, event | category | flops | bytes accessed | tf_op | source)
XLA Modules:
  0.0 191.9 jit_solution(4200899454557848053)
XLA Ops:
  7.2 0.0 copy-start
  7.2 0.0 copy-start.1
  7.2 0.0 all-reduce.3.cloned.1.call-start
  7.2 1.3 copy-done
  8.6 0.0 copy-start.9
  8.6 3.4 %fusion.17 = f32[640,256]{1,0:T(8,128)S(1)} fusion(bf16[640,3072]{1,0:T(8,128)(2,1)} %param.11, bf16[3072,256]{1,0:T(8,128)(2,1)S(1)} %copy-done), kind=kOutput, calls=%fused_computation.48 | convolution fusion | flops 1006632960 | bytes 6160384 | tf_op jit(solution)/shard_map/dot_general | solution.py:66
  12.0 0.0 copy-done.1
  12.1 0.0 copy-start.8
  12.1 0.4 fusion.5
  12.5 1.2 convolution_add_fusion
  13.7 0.0 copy-done.9
  13.7 0.0 copy-done.8
  13.7 1.2 fusion.16
  14.9 0.0 copy-done.4
  14.9 0.0 copy-start.7
  14.9 0.3 fusion.8
  15.2 1.0 convolution_add_fusion.1
  16.2 0.0 all-reduce.3.cloned.1.call-update
  16.2 0.0 all-gather.2.cloned.1.call-start
  16.3 78.1 %all-reduce.3.cloned.1.call-done = (f32[256,256]{1,0:T(8,128)}, f32[256,512]{1,0:T(8,128)}) async-done(((f32[256,256]{1,0:T(8,128)}, f32[256,512]{1,0:T(8,128)}), (f32[256,256]{1,0:T(8,128)}, f32[256,512]{1,0:T(8,128)})) %all-reduce.3.cloned.1.call-update) | async-done | bytes 786448 | tf_op jit(solution)/shard_map/psum | solution.py:68
  94.4 0.0 copy-done.7
  94.4 2.1 %multiply_reduce_fusion = (f32[]{:T(128)}, f32[256,512]{1,0:T(8,128)S(1)}, f32[256,512]{1,0:T(8,128)S(1)}) fusion(f32[256,512]{1,0:T(8,128)} %get-tuple-element.11, f32[256,512]{1,0:T(8,128)S(1)} %copy-done.7, f32[256,512]{1,0:T(8,128)} %param.20), kind=kLoop, calls=%fused_computation.9 | loop fusion | flops 1441791 | bytes 2621444 | tf_op jit(solution)/shard_map/reduce_sum | solution.py:73
  96.5 2.3 %multiply_reduce_fusion.1 = (f32[]{:T(128)}, f32[256,256]{1,0:T(8,128)S(1)}, f32[256,256]{1,0:T(8,128)S(1)}) fusion(f32[256,256]{1,0:T(8,128)} %get-tuple-element.10, f32[256,256]{1,0:T(8,128)} %param.19, f32[256,256]{1,0:T(8,128)} %param.18), kind=kLoop, calls=%fused_computation.15 | loop fusion | flops 720895 | bytes 1310724 | tf_op jit(solution)/shard_map/reduce_sum | solution.py:73
  100.1 6.2 %psum.23 = f32[]{:T(128)} all-reduce(f32[]{:T(128)S(6)} %add.71), channel_id=1, replica_groups=mesh['fs'=4,'rep'=2,'tp'=4] {'tp'}, use_global_device_ids=true, to_apply=%region_4.0 | all-reduce | flops 1 | bytes 8 | tf_op jit(solution)/shard_map/psum | solution.py:74
  107.0 3.2 %fusion.12 = (bf16[384,512]{1,0:T(8,128)(2,1)}, f32[384,512]{1,0:T(8,128)}, f32[384,512]{1,0:T(8,128)}) fusion(f32[384,512]{1,0:T(8,128)} %param.17, f32[256,512]{1,0:T(8,128)S(1)} %get-tuple-element.38, f32[256,512]{1,0:T(8,128)S(1)} %get-tuple-element.39, bf16[3072,256]{1,0:T(8,128)(2,1)S(1)} %copy-done, s32[]{:T(128)S(6)} %select_n.17, f32[]{:T(128)S(6)} %sqrt.11), kind=kOutput, calls=%fused_computation.45 | convolution fusion | flops 605028352 | bytes 3997704 | tf_op jit(solution)/shard_map/dot_general | solution.py:78
  110.2 0.0 all-gather.2.cloned.1.call-update
  110.2 2.4 %fusion.13 = (bf16[384,256]{1,0:T(8,128)(2,1)S(1)}, f32[384,256]{1,0:T(8,128)}, f32[384,256]{1,0:T(8,128)}) fusion(f32[384,256]{1,0:T(8,128)} %param.16, f32[256,256]{1,0:T(8,128)S(1)} %get-tuple-element.36, f32[256,256]{1,0:T(8,128)S(1)} %get-tuple-element.37, bf16[3072,256]{1,0:T(8,128)(2,1)} %param.14, s32[]{:T(128)S(6)} %select_n.17, f32[]{:T(128)S(6)} %sqrt.11), kind=kOutput, calls=%fused_computation.46 | convolution fusion | flops 302514176 | bytes 2097160 | tf_op jit(solution)/shard_map/dot_general | solution.py:77
  112.6 0.0 copy-done.2
  112.6 0.0 copy-done.3
  112.6 0.0 copy-done.5
  112.6 0.0 copy-done.6
  112.6 0.9 collective-permute-start
  113.5 8.7 %collective-permute-done = bf16[384,256]{1,0:T(8,128)(2,1)S(1)} collective-permute-done((bf16[384,256]{1,0:T(8,128)(2,1)S(1)}, bf16[384,256]{1,0:T(8,128)(2,1)S(1)}, u32[]{:S(2)}, u32[]{:S(2)}) %collective-permute-start) | collective-permute-done | bytes 196640 | tf_op jit(solution)/shard_map/ppermute | solution.py:22
  122.2 0.0 collective-permute-start.1
  122.2 4.7 %collective-permute-start.4 = (bf16[384,256]{1,0:T(8,128)(2,1)S(1)}, bf16[384,256]{1,0:T(8,128)(2,1)S(1)}, u32[]{:S(2)}, u32[]{:S(2)}) collective-permute-start(bf16[384,256]{1,0:T(8,128)(2,1)S(1)} %get-tuple-element.14), channel_id=1, source_target_pairs={{0,28},{4,0},{8,4},{12,8},{16,12},{20,16},{24,20},{28,24},{1,29},{... | collective-permute-start | bytes 589832 | tf_op jit(solution)/shard_map/ppermute | solution.py:24
  126.9 9.3 %collective-permute-done.1 = bf16[384,256]{1,0:T(8,128)(2,1)S(1)} collective-permute-done((bf16[384,256]{1,0:T(8,128)(2,1)S(1)}, bf16[384,256]{1,0:T(8,128)(2,1)S(1)}, u32[]{:S(2)}, u32[]{:S(2)}) %collective-permute-start.1) | collective-permute-done | bytes 196640 | tf_op jit(solution)/shard_map/ppermute | solution.py:22
  136.2 0.0 collective-permute-start.2
  136.2 0.0 collective-permute-done.4
  136.2 4.7 %collective-permute-start.5 = (bf16[384,256]{1,0:T(8,128)(2,1)S(1)}, bf16[384,256]{1,0:T(8,128)(2,1)S(1)}, u32[]{:S(2)}, u32[]{:S(2)}) collective-permute-start(bf16[384,256]{1,0:T(8,128)(2,1)S(1)} %collective-permute-done.4), channel_id=1, source_target_pairs={{0,28},{4,0},{8,4},{12,8},{16,12},{20,16},{24,20},{28,24},{1,29},{... | collective-permute-start | bytes 589832 | tf_op jit(solution)/shard_map/ppermute | solution.py:24
  140.9 3.6 %collective-permute-done.2 = bf16[384,256]{1,0:T(8,128)(2,1)S(1)} collective-permute-done((bf16[384,256]{1,0:T(8,128)(2,1)S(1)}, bf16[384,256]{1,0:T(8,128)(2,1)S(1)}, u32[]{:S(2)}, u32[]{:S(2)}) %collective-permute-start.2) | collective-permute-done | bytes 196640 | tf_op jit(solution)/shard_map/ppermute | solution.py:22
  144.6 1.4 collective-permute-start.3
  145.9 1.4 collective-permute-done.5
  147.3 2.2 %collective-permute-start.6 = (bf16[384,256]{1,0:T(8,128)(2,1)S(1)}, bf16[384,256]{1,0:T(8,128)(2,1)S(1)}, u32[]{:S(2)}, u32[]{:S(2)}) collective-permute-start(bf16[384,256]{1,0:T(8,128)(2,1)S(1)} %collective-permute-done.5), channel_id=1, source_target_pairs={{0,28},{4,0},{8,4},{12,8},{16,12},{20,16},{24,20},{28,24},{1,29},{... | collective-permute-start | bytes 589832 | tf_op jit(solution)/shard_map/ppermute | solution.py:24
  149.5 4.5 %collective-permute-done.3 = bf16[384,256]{1,0:T(8,128)(2,1)S(1)} collective-permute-done((bf16[384,256]{1,0:T(8,128)(2,1)S(1)}, bf16[384,256]{1,0:T(8,128)(2,1)S(1)}, u32[]{:S(2)}, u32[]{:S(2)}) %collective-permute-start.3) | collective-permute-done | bytes 196640 | tf_op jit(solution)/shard_map/ppermute | solution.py:22
  154.2 5.2 %collective-permute-done.6 = bf16[384,256]{1,0:T(8,128)(2,1)S(1)} collective-permute-done((bf16[384,256]{1,0:T(8,128)(2,1)S(1)}, bf16[384,256]{1,0:T(8,128)(2,1)S(1)}, u32[]{:S(2)}, u32[]{:S(2)}) %collective-permute-start.6) | collective-permute-done | bytes 196640 | tf_op jit(solution)/shard_map/ppermute | solution.py:24
  159.6 1.5 constant_dynamic-slice_fusion
  161.1 20.2 %all-gather.2.cloned.1.call-done = bf16[3072,512]{1,0:T(8,128)(2,1)} async-done(((bf16[384,512]{1,0:T(8,128)(2,1)}), bf16[3072,512]{1,0:T(8,128)(2,1)}) %all-gather.2.cloned.1.call-update) | async-done | bytes 3145744 | tf_op jit(solution)/shard_map/all_gather | solution.py:83
  181.4 3.8 %copy.39 = bf16[3072,512]{1,0:T(8,128)(2,1)} copy(bf16[3072,512]{1,0:T(8,128)(2,1)} %all-gather.2.cloned.1.call-done) | data formatting | bytes 6291456
  (21 shorter events, 0.2 us)
Async XLA Ops:
  7.2 1.4 copy-start
  7.2 4.9 %copy-start.1 = (bf16[640,512]{1,0:T(8,128)(2,1)S(1)}, bf16[640,512]{1,0:T(8,128)(2,1)}, u32[]{:S(2)}) copy-start(bf16[640,512]{1,0:T(8,128)(2,1)} %param.13) | copy-start | bytes 1966084
  7.2 87.2 %all-reduce.3.cloned.1.call-start = ((), (), s32[]{:S(2)}) async-start(), calls=%async_computation.1 | async-start | bytes 1572864 | tf_op jit(solution)/shard_map/psum | solution.py:68
  8.6 5.1 %copy-start.9 = (bf16[640,3072]{1,0:T(8,128)(2,1)S(1)}, bf16[640,3072]{1,0:T(8,128)(2,1)}, u32[]{:S(2)}) copy-start(bf16[640,3072]{1,0:T(8,128)(2,1)} %param.11) | copy-start | bytes 11796484
  12.1 1.6 copy-start.8
  13.7 1.2 copy-start.4
  14.9 79.5 %copy-start.7 = (f32[256,512]{1,0:T(8,128)S(1)}, f32[256,512]{1,0:T(8,128)}, u32[]{:S(2)}) copy-start(f32[256,512]{1,0:T(8,128)} %param.21) | copy-start | bytes 1572868
  16.2 165.1 %all-gather.2.cloned.1.call-start = ((), (), s32[]{:S(2)}) async-start(), calls=%async_computation | async-start | bytes 3538944 | tf_op jit(solution)/shard_map/all_gather | solution.py:83
  96.5 16.1 %copy-start.2 = (f32[256,512]{1,0:T(8,128)}, f32[256,512]{1,0:T(8,128)S(1)}, u32[]{:S(2)}) copy-start(f32[256,512]{1,0:T(8,128)S(1)} %get-tuple-element.39) | copy-start | bytes 1572868
  96.5 16.1 %copy-start.3 = (f32[256,512]{1,0:T(8,128)}, f32[256,512]{1,0:T(8,128)S(1)}, u32[]{:S(2)}) copy-start(f32[256,512]{1,0:T(8,128)S(1)} %get-tuple-element.38) | copy-start | bytes 1572868
  98.8 13.8 %copy-start.5 = (f32[256,256]{1,0:T(8,128)}, f32[256,256]{1,0:T(8,128)S(1)}, u32[]{:S(2)}) copy-start(f32[256,256]{1,0:T(8,128)S(1)} %get-tuple-element.37) | copy-start | bytes 786436
  98.8 13.8 %copy-start.6 = (f32[256,256]{1,0:T(8,128)}, f32[256,256]{1,0:T(8,128)S(1)}, u32[]{:S(2)}) copy-start(f32[256,256]{1,0:T(8,128)S(1)} %get-tuple-element.36) | copy-start | bytes 786436
  112.6 9.5 %collective-permute-start = (bf16[384,256]{1,0:T(8,128)(2,1)S(1)}, bf16[384,256]{1,0:T(8,128)(2,1)S(1)}, u32[]{:S(2)}, u32[]{:S(2)}) collective-permute-start(bf16[384,256]{1,0:T(8,128)(2,1)S(1)} %get-tuple-element.14), channel_id=1, source_target_pairs={{0,4},{4,8},{8,12},{12,16},{16,20},{20,24},{24,28},{28,0},{1,5},{5... | collective-permute-start | bytes 589832 | tf_op jit(solution)/shard_map/ppermute | solution.py:22
  122.2 14.0 %collective-permute-start.1 = (bf16[384,256]{1,0:T(8,128)(2,1)S(1)}, bf16[384,256]{1,0:T(8,128)(2,1)S(1)}, u32[]{:S(2)}, u32[]{:S(2)}) collective-permute-start(bf16[384,256]{1,0:T(8,128)(2,1)S(1)} %collective-permute-done), channel_id=1, source_target_pairs={{0,4},{4,8},{8,12},{12,16},{16,20},{20,24},{24,28},{28,0},{1,5},{5... | collective-permute-start | bytes 589832 | tf_op jit(solution)/shard_map/ppermute | solution.py:22
  122.2 14.0 %collective-permute-start.4 = (bf16[384,256]{1,0:T(8,128)(2,1)S(1)}, bf16[384,256]{1,0:T(8,128)(2,1)S(1)}, u32[]{:S(2)}, u32[]{:S(2)}) collective-permute-start(bf16[384,256]{1,0:T(8,128)(2,1)S(1)} %get-tuple-element.14), channel_id=1, source_target_pairs={{0,28},{4,0},{8,4},{12,8},{16,12},{20,16},{24,20},{28,24},{1,29},{... | collective-permute-start | bytes 589832 | tf_op jit(solution)/shard_map/ppermute | solution.py:24
  136.2 8.4 %collective-permute-start.2 = (bf16[384,256]{1,0:T(8,128)(2,1)S(1)}, bf16[384,256]{1,0:T(8,128)(2,1)S(1)}, u32[]{:S(2)}, u32[]{:S(2)}) collective-permute-start(bf16[384,256]{1,0:T(8,128)(2,1)S(1)} %collective-permute-done.1), channel_id=1, source_target_pairs={{0,4},{4,8},{8,12},{12,16},{16,20},{20,24},{24,28},{28,0},{1,5},{5... | collective-permute-start | bytes 589832 | tf_op jit(solution)/shard_map/ppermute | solution.py:22
  136.2 11.1 %collective-permute-start.5 = (bf16[384,256]{1,0:T(8,128)(2,1)S(1)}, bf16[384,256]{1,0:T(8,128)(2,1)S(1)}, u32[]{:S(2)}, u32[]{:S(2)}) collective-permute-start(bf16[384,256]{1,0:T(8,128)(2,1)S(1)} %collective-permute-done.4), channel_id=1, source_target_pairs={{0,28},{4,0},{8,4},{12,8},{16,12},{20,16},{24,20},{28,24},{1,29},{... | collective-permute-start | bytes 589832 | tf_op jit(solution)/shard_map/ppermute | solution.py:24
  144.6 9.5 %collective-permute-start.3 = (bf16[384,256]{1,0:T(8,128)(2,1)S(1)}, bf16[384,256]{1,0:T(8,128)(2,1)S(1)}, u32[]{:S(2)}, u32[]{:S(2)}) collective-permute-start(bf16[384,256]{1,0:T(8,128)(2,1)S(1)} %collective-permute-done.2), channel_id=1, source_target_pairs={{0,4},{4,8},{8,12},{12,16},{16,20},{20,24},{24,28},{28,0},{1,5},{5... | collective-permute-start | bytes 589832 | tf_op jit(solution)/shard_map/ppermute | solution.py:22
  147.3 12.1 %collective-permute-start.6 = (bf16[384,256]{1,0:T(8,128)(2,1)S(1)}, bf16[384,256]{1,0:T(8,128)(2,1)S(1)}, u32[]{:S(2)}, u32[]{:S(2)}) collective-permute-start(bf16[384,256]{1,0:T(8,128)(2,1)S(1)} %collective-permute-done.5), channel_id=1, source_target_pairs={{0,28},{4,0},{8,4},{12,8},{16,12},{20,16},{24,20},{28,24},{1,29},{... | collective-permute-start | bytes 589832 | tf_op jit(solution)/shard_map/ppermute | solution.py:24
Sparse Core Ops, SparseCore 0:
  16.4 77.9 all-reduce.2
  110.3 71.0 all-gather.1
